TPU v7x, 128 devices: a whole 4x4x4 slice. The times are simulated.
128 devices in a mesh: fs: 16 (over z, y), tp: 8 (over x, core).
Axes of the slice: x: 4, y: 4, z: 4, core: 2. Of those that a mesh axis runs over, the one named last changes fastest.
Arguments:
- tokens: bfloat16 [32768, 2048], P('fs'), may hold values from -6 to 6
- norm_gain: float32 [2048], replicated, may hold values from 0.1 to 1.9
- gate_weight: bfloat16 [2048, 5632], P('fs', 'tp'), may hold values from -0.125 to 0.125
- up_weight: bfloat16 [2048, 5632], P('fs', 'tp'), may hold values from -0.125 to 0.125
- down_weight: bfloat16 [5632, 2048], P('tp', 'fs'), may hold values from -0.078125 to 0.078125
Outputs:
- mixed: bfloat16 [32768, 2048], P(('fs', 'tp'))
All inputs are finite; a program needn't handle non-finite values.
Results may differ from a plain program's by a relative error of at most 0.014.
Values may be sent and summed in bfloat16 or wider, within the bound.
A program may use at most 128 MiB of HBM per device.

v0:
```python
import jax
import jax.numpy as jnp
from jax import lax
from jax.sharding import PartitionSpec as P


def side_by_side(arrays, axis, dim, along):
    widths = [a.shape[along] for a in arrays]
    both = jnp.concatenate(arrays, axis=along)
    whole = lax.all_gather(both, axis, axis=dim, tiled=True)
    return tuple(jnp.split(whole, [sum(widths[:k]) for k in range(1, len(widths))], axis=along))


def from_everyone(value, axis):
    copies = jnp.broadcast_to(value, (lax.axis_size(axis), *value.shape))
    return lax.all_to_all(copies, axis, split_axis=0, concat_axis=0, tiled=True)


def laid_out(blocks, dim):
    shape = list(blocks.shape[1:])
    shape[dim] *= blocks.shape[0]
    return jnp.moveaxis(blocks, 0, dim).reshape(shape)


def gathered_copies(value, axis, dim):
    blocks = from_everyone(value, axis)
    return laid_out(blocks, dim)


def per_device(tokens, norm_gain, gate_weight, up_weight, down_weight):
    xf = tokens.astype(jnp.float32)
    scale = lax.rsqrt(jnp.mean(xf * xf, axis=-1, keepdims=True) + 1e-06)
    normed = (xf * scale * norm_gain).astype(jnp.bfloat16)
    gate_full, up_full = side_by_side((gate_weight, up_weight), "fs", 0, 1)
    gate = jnp.dot(normed, gate_full, preferred_element_type=jnp.float32)
    up = jnp.dot(normed, up_full, preferred_element_type=jnp.float32)
    hidden = (jax.nn.silu(gate) * up).astype(jnp.bfloat16)
    down_full = gathered_copies(down_weight, "fs", 1)
    return lax.psum_scatter(
        jnp.dot(hidden, down_full, preferred_element_type=jnp.float32).astype(jnp.bfloat16),
        "tp",
        scatter_dimension=0,
        tiled=True,
    )


def solution(mesh):
    placed = (P("fs", None), P(), P("fs", "tp"), P("fs", "tp"), P("tp", "fs"))
    return jax.shard_map(
        per_device, mesh=mesh, in_specs=placed, out_specs=P(("fs", "tp"), None), check_vma=False
    )
```

profile of v0, /device:TPU:1, one launch (start us, length us, event | category | flops | bytes accessed | tf_op | source)
XLA Modules:
  0.0 192.2 jit_solution(17103997552498888308)
XLA Ops:
  6.5 0.0 all-gather.2.cloned.1.call-start
  6.5 1.8 pad_maximum_fusion
  8.3 0.0 all-gather.2.cloned.1.call-update
  8.3 3.1 %broadcast_in_dim.2 = bf16[16,704,128]{2,1,0:T(8,128)(2,1)} broadcast(bf16[704,128]{1,0:T(8,128)(2,1)} %param.9), dimensions={1,2} | broadcast | bytes 3063808 | tf_op jit(solution)/shard_map/broadcast_in_dim | solution.py:15
  11.4 0.0 copy-start
  11.4 8.7 %all-to-all-start = ((bf16[16,704,128]{2,1,0:T(8,128)(2,1)}), bf16[16,704,128]{2,1,0:T(8,128)(2,1)S(1)}, u32[]{:S(2)}, u32[]{:S(2)}) async-start(bf16[16,704,128]{2,1,0:T(8,128)(2,1)} %broadcast_in_dim.2), calls=%async_computation | async-start | bytes 5767168 | tf_op jit(solution)/shard_map/all_to_all | solution.py:16
  20.1 0.0 reduce-scatter.2.cloned.1.call-start
  20.2 5.3 %fusion = f32[2048]{0:T(1024)S(1)} fusion(bf16[2048,2048]{1,0:T(8,128)(2,1)} %param.5), kind=kLoop, calls=%fused_computation.2 | loop fusion | flops 12580864 | bytes 8396800 | tf_op jit(solution)/shard_map/reduce_sum | solution.py:32
  25.5 76.7 %all-gather.2.cloned.1.call-done = bf16[2048,1408]{0,1:T(8,128)(2,1)} async-done(((bf16[128,1408]{0,1:T(8,128)(2,1)}), bf16[2048,1408]{0,1:T(8,128)(2,1)}) %all-gather.2.cloned.1.call-update) | async-done | bytes 5767184 | tf_op jit(solution)/shard_map/all_gather | solution.py:10
  102.2 0.0 copy-done
  102.2 11.2 %fusion.7 = f32[2048,704]{0,1:T(8,128)} fusion(bf16[2048,1408]{0,1:T(8,128)(2,1)} %all-gather.2.cloned.1.call-done, bf16[2048,2048]{1,0:T(8,128)(2,1)} %param.5, f32[2048]{0:T(1024)S(1)} %copy-done, f32[2048]{0:T(1024)S(1)} %add_rsqrt_fusion), kind=kOutput, calls=%fused_computation.10 | convolution fusion | flops 5922357248 | bytes 17055744 | tf_op jit(solution)/shard_map/dot_general | solution.py:35
  113.4 0.0 all-to-all-done
  113.4 19.3 %convolution_convert_fusion = bf16[2048,2048]{1,0:T(8,128)(2,1)} fusion(f32[2048,704]{0,1:T(8,128)} %fusion.7, bf16[2048,1408]{0,1:T(8,128)(2,1)} %all-gather.2.cloned.1.call-done, bf16[2048,2048]{1,0:T(8,128)(2,1)} %param.5, f32[2048]{0:T(1024)S(1)} %copy-done, f32[2048]{0:T(1024)S(1)} %add_rsqrt_fusion, bf16[16,704,128]{2,1,0:T(8,128)(2,1)S(1)} %all-to-all-done), kind=kOutput, calls=%fused_computation.5 | convolution fusion | flops 11840782336 | bytes 28327936 | tf_op jit(solution)/shard_map/dot_general | solution.py:40
  132.7 0.0 reduce-scatter.2.cloned.1.call-update
  132.7 52.6 %reduce-scatter.2.cloned.1.call-done = bf16[256,2048]{1,0:T(8,128)(2,1)} async-done(((bf16[2048,2048]{1,0:T(8,128)(2,1)}), bf16[256,2048]{1,0:T(8,128)(2,1)}) %reduce-scatter.2.cloned.1.call-update) | async-done | bytes 1048592 | tf_op jit(solution)/shard_map/reduce_scatter | solution.py:39
  (1 shorter events, 0.0 us)
Async XLA Ops:
  6.5 95.7 %all-gather.2.cloned.1.call-start = ((), (), s32[]{:S(2)}) async-start(), calls=%async_computation.2 | async-start | bytes 6127616 | tf_op jit(solution)/shard_map/all_gather | solution.py:10
  11.4 90.8 %copy-start = (f32[2048]{0:T(1024)S(1)}, f32[2048]{0:T(1024)}, u32[]{:S(2)}) copy-start(f32[2048]{0:T(1024)} %param.6) | copy-start | bytes 24580
  11.4 102.0 %all-to-all-start = ((bf16[16,704,128]{2,1,0:T(8,128)(2,1)}), bf16[16,704,128]{2,1,0:T(8,128)(2,1)S(1)}, u32[]{:S(2)}, u32[]{:S(2)}) async-start(bf16[16,704,128]{2,1,0:T(8,128)(2,1)} %broadcast_in_dim.2), calls=%async_computation | async-start | bytes 5767168 | tf_op jit(solution)/shard_map/all_to_all | solution.py:16
  20.1 165.3 %reduce-scatter.2.cloned.1.call-start = ((), (), s32[]{:S(2)}) async-start(), calls=%async_computation.3 | async-start | bytes 9437184 | tf_op jit(solution)/shard_map/reduce_scatter | solution.py:39
Sparse Core Ops, SparseCore 0:
  9.4 92.7 all-gather.1
  132.9 52.4 reduce-scatter.1
where the time goes:
time: 192 us
  waiting for transfers between devices  129 us (67%)
  matrix products  30.5 us (16%)
  between operations  13.4 us (7%)
  starting transfers between devices  8.76 us (5%)
  other arithmetic  7.1 us (4%)
  local copies, waits for them, and re-layouts  3.06 us (2%)
    all_gather x1, waiting for transfers between devices, side_by_side(): whole = lax.all_gather(both, axis, axis=dim, tiled=True)  76.7 us
    reduce_scatter x1, waiting for transfers between devices, per_device(): lax.psum_scatter(jnp.dot(hidden, down_full, preferred_element_type=jnp.fl...  52.6 us
    dot_general x1, matrix products, per_device(): jnp.dot(hidden, down_full, preferred_element_type=jnp.float32)  19.3 us
    dot_general x1, matrix products, per_device(): gate = jnp.dot(normed, gate_full, preferred_element_type=jnp.float32)  11.2 us
    all_to_all x1, starting transfers between devices, from_everyone(): return lax.all_to_all(copies, axis, split_axis=0, concat_axis=0, tiled=True)  8.72 us
    reduce_sum x1, other arithmetic, per_device(): scale = lax.rsqrt(jnp.mean(xf * xf, axis=-1, keepdims=True) + 1e-06)  5.32 us
  transfers between devices with their start and end apart: 3, of which 2 were waited for; matrix products, arithmetic and copies ran while one was open for 10% of the time, Pallas kernels for 0%

commit v1 on v0

v1 whole, which is shorter than its diff:
```python
import heapq

import jax
import jax.numpy as jnp
from jax import lax
from jax.experimental import pallas as pl
from jax.experimental.pallas import tpu as pltpu
from jax.sharding import PartitionSpec as P

D = 2048
N_FS = 16
F = 704
FM = 640
TT = 256
GQ = 32
DQ = 176
LINKS = ("y+", "y-", "z+", "z-")
FIRST = {"y+": (0, 1, 2, 3), "y-": (1, 0, 3, 2), "z+": (2, 3, 0, 1), "z-": (3, 2, 1, 0)}


def near(d):
    return (d + 1) % 4 - 1


def onward(q, dz, dy):
    first, second = ("y", "z") if q < 2 else ("z", "y")
    sign = "+" if q % 2 == 0 else "-"
    a, b = (dy, dz) if q < 2 else (dz, dy)
    came = {-1: "+", 1: "-"}
    if b == 0:
        out = [first + sign] if came.get(a) == sign else []
        return out + [second + sign, second + ("-" if sign == "+" else "+")]
    return [second + sign] if came.get(b) == sign else []


def seen_from(link, dz, dy):
    step = 1 if link[1] == "+" else -1
    return (near(dz - step), dy) if link[0] == "z" else (dz, near(dy - step))


def gather_events(unit, lat, backlog):
    free = {l: 0.0 for l in LINKS}
    count = {l: 0 for l in LINKS}
    heap = {l: [] for l in LINKS}
    flying, n = [], 0

    def offer(l, k, q, dz, dy):
        nonlocal n
        n += 1
        heapq.heappush(heap[l], (k == "d", n, k, q, dz, dy))

    def top_up(t):
        nonlocal n
        sends = []
        for l in LINKS:
            while heap[l] and free[l] - t < backlog and (heap[l][0][2] == "g" or count[l] >= 15):
                _, _, k, q, dz, dy = heapq.heappop(heap[l])
                count[l] += 1
                n += 1
                free[l] = max(t, free[l]) + unit[k]
                sends.append((l, k, q, dz, dy))
                heapq.heappush(flying, (free[l] + lat, n, k, q, *seen_from(l, dz, dy)))
        return sends

    for l in LINKS:
        for k in "gd":
            for q in FIRST[l]:
                offer(l, k, q, 0, 0)
    events = [(0.0, None, top_up(0.0))]
    while flying:
        t, _, k, q, dz, dy = heapq.heappop(flying)
        for l in onward(q, dz, dy):
            offer(l, k, q, dz, dy)
        events.append((t, (k, q, dz, dy), top_up(t)))
    return events


def make_plan(unit={"g": 1.93, "d": 0.97}, lat=2.0, backlog=6.0, sib=1.8):
    events = gather_events(unit, lat, backlog)
    done, left = {("g", 0, 0): 0.0, ("d", 0, 0): 0.0}, {}
    for t, what, _ in events[1:]:
        k, q, dz, dy = what
        left[(k, dz, dy)] = left.get((k, dz, dy), 0) + 1
        if left[(k, dz, dy)] == 4:
            done[(k, dz, dy)] = t
    order = {k: [key[1:] for key in sorted((key for key in done if key[0] == k), key=lambda key: done[key])] for k in "gd"}
    assert len(order["g"]) == 16 and len(order["d"]) == 16
    steps = [order["g"][4 * i : 4 * i + 4] for i in range(4)]
    groups = [order["d"][:1]] + [order["d"][1 + 2 * i : 3 + 2 * i] for i in range(7)] + [order["d"][15:]]
    work = [(1.5, 1.2, ("norm", b)) for b in range(4)]
    for i in range(3):
        ready = max(done[("g", *s)] for s in steps[i])
        work.append((ready, 2.2, ("acc", i, 0)))
        work.append((ready + sib, 2.2, ("acc", i, 1)))
        work.append((ready + sib, 0.5, ("acc", i, 2)))
    ready = max(done[("g", *s)] for s in steps[3]) + sib
    for b in range(4):
        work += [(ready, 1.2, ("fin", b)), (ready, 0.3, ("down", 0, b))]
    for i in range(1, len(groups)):
        ready = max(done[("d", *s)] for s in groups[i]) + sib
        work += [(ready, 0.4, ("down", i, b)) for b in range(4)]
    plan, now, w, got = [], 0.0, 0, {}
    plan += [("send", *s) for s in events[0][2]] + [("pass", "g", 0, 0), ("pass", "d", 0, 0)]
    for t, what, sends in events[1:]:
        while w < len(work) and max(now, work[w][0]) + work[w][1] <= t + 0.6:
            plan.append(work[w][2])
            now = max(now, work[w][0]) + work[w][1]
            w += 1
        k, q, dz, dy = what
        plan.append(("recv", *what))
        now = max(now, t)
        plan += [("send", *s) for s in sends]
        got[(k, dz, dy)] = got.get((k, dz, dy), 0) + 1
        if got[(k, dz, dy)] == 4:
            plan.append(("pass", k, dz, dy))
    plan += [item[2] for item in work[w:]]
    return plan, steps, groups


def kernel(tok_hbm, gain_ref, gu_hbm, dn_hbm, out_ref, tok, normed, wgu, wdn, acc, hid, far_s, far_r, near_p, near_m,
           in_m, in_n, own, loc_sem, tok_sem, g_recv, d_recv, gs_recv, ds_recv, x_recv, send_sem):
    plan, steps, groups = make_plan()
    fs, tp = lax.axis_index("fs"), lax.axis_index("tp")
    z, y = fs // 4, fs % 4
    x, core = tp // 2, tp % 2

    def dev(link):
        step = 1 if link[1] == "+" else 3
        if link[0] == "z":
            return {"fs": ((z + step) % 4) * 4 + y, "tp": tp}
        if link[0] == "y":
            return {"fs": z * 4 + (y + step) % 4, "tp": tp}
        if link[0] == "x":
            return {"fs": fs, "tp": ((x + step) % 4) * 2 + core}
        return {"fs": fs, "tp": x * 2 + 1 - core}

    peers = {l: dev(l) for l in LINKS + ("x+", "x-", "c+")}
    shard = {(dz, dy): ((z + dz + 4) % 4) * 4 + (y + dy + 4) % 4 for dz in range(-1, 3) for dy in range(-1, 3)}

    def label(dz, dy):
        return (dz + 1) * 4 + dy + 1

    def rows(dz, dy, at, size):
        return pl.ds(pl.multiple_of(shard[(dz, dy)] * 128 + at, size), size)

    def piece(k, q, dz, dy):
        if k == "g":
            return wgu.at[0, rows(dz, dy, q * GQ, GQ), :]
        return wdn.at[shard[(dz, dy)], 0, pl.ds(q * DQ, DQ), :]

    def copy_piece(link, k, q, dz, dy):
        there = seen_from(link, dz, dy)
        ref = piece(k, q, dz, dy)
        sems, s = (g_recv, 0) if k == "g" else (d_recv, 1)
        return pltpu.make_async_remote_copy(
            src_ref=ref, dst_ref=ref, send_sem=send_sem.at[s], recv_sem=sems.at[q * 16 + label(*there)],
            device_id=peers[link], device_id_type=pl.DeviceIdType.MESH)

    def recv_piece(k, q, dz, dy):
        ref = piece(k, q, dz, dy)
        sem = (g_recv if k == "g" else d_recv).at[q * 16 + label(dz, dy)]
        pltpu.make_async_copy(ref, ref, sem).wait()

    def whole(k, slot, dz, dy):
        if k == "g":
            return wgu.at[slot, rows(dz, dy, 0, 128), :]
        return wdn.at[shard[(dz, dy)], slot]

    def pass_shard(k, dz, dy):
        sems, s = (gs_recv, 2) if k == "g" else (ds_recv, 3)
        pltpu.make_async_remote_copy(
            src_ref=whole(k, 0, dz, dy), dst_ref=whole(k, 1, dz, dy), send_sem=send_sem.at[s],
            recv_sem=sems.at[label(dz, dy)], device_id=peers["c+"], device_id_type=pl.DeviceIdType.MESH).start()

    passed = set()

    def need_passed(k, shards):
        for s in shards:
            if (k, *s) not in passed:
                passed.add((k, *s))
                ref = whole(k, 1, *s)
                pltpu.make_async_copy(ref, ref, (gs_recv if k == "g" else ds_recv).at[label(*s)]).wait()

    own_g = pltpu.make_async_copy(gu_hbm, whole("g", 0, 0, 0), loc_sem.at[0])
    own_d = pltpu.make_async_copy(dn_hbm, whole("d", 0, 0, 0), loc_sem.at[1])
    own_g.start()
    own_d.start()

    def tok_copy(b):
        to = (x + (2, 1, 3, 0)[b]) % 4
        at = pl.multiple_of((to * 2 + core) * TT, TT)
        return pltpu.make_async_copy(tok_hbm.at[pl.ds(at, TT), :], tok.at[b], tok_sem.at[b])

    for b in range(4):
        tok_copy(b).start()

    barrier = pltpu.get_barrier_semaphore()
    for peer in peers.values():
        pl.semaphore_signal(barrier, inc=1, device_id=peer, device_id_type=pl.DeviceIdType.MESH)
    pl.semaphore_wait(barrier, len(peers))
    own_g.wait()
    own_d.wait()

    def norm(b):
        tok_copy(b).wait()

        @pl.loop(0, TT // 16)
        def _(i):
            r = pl.ds(pl.multiple_of(i * 16, 16), 16)
            v = tok[b, r, :].astype(jnp.float32)
            scale = lax.rsqrt(jnp.mean(v * v, axis=-1, keepdims=True) + 1e-06)
            n = (v * scale * gain_ref[...]).astype(jnp.bfloat16)
            to = pl.ds(pl.multiple_of(b * TT + i * 16, 16), 16)
            for s in range(N_FS):
                normed[s, to, :] = n[:, s * 128 : (s + 1) * 128]

    def lhs(step, r):
        return jnp.concatenate([normed[shard[s], r, :] for s in step], axis=1)

    def rhs(step, tile):
        def part(s):
            if tile < 10:
                return wgu[tile // 5, rows(*s, 0, 128), (tile % 5) * 256 : (tile % 5) * 256 + 256]
            return jnp.concatenate([wgu[c, rows(*s, 0, 128), 2 * FM : 2 * F] for c in range(2)], axis=1)

        return jnp.concatenate([part(s) for s in step], axis=0)

    def accumulate(i, part):
        step = steps[i]
        if part > 0:
            need_passed("g", step)
        tiles = (range(0, 5), range(5, 10), range(10, 11))[part]

        @pl.loop(0, 2)
        def _(h):
            r = pl.ds(pl.multiple_of(h * 512, 512), 512)
            left = lhs(step, r)
            for tile in tiles:
                prod = jnp.dot(left, rhs(step, tile), preferred_element_type=jnp.float32)
                if i == 0:
                    acc[tile, r, :] = prod
                else:
                    acc[tile, r, :] += prod

    def gated(g, u):
        return (g / (1.0 + jnp.exp(-g)) * u).astype(jnp.bfloat16)

    def finish(b):
        need_passed("g", steps[3])
        r = pl.ds(b * TT, TT)
        left = lhs(steps[3], r)
        for tile in range(11):
            v = acc[tile, r, :] + jnp.dot(left, rhs(steps[3], tile), preferred_element_type=jnp.float32)
            a, c = v[:, :128], v[:, 128:]
            if tile == 10:
                low = lax.broadcasted_iota(jnp.int32, a.shape, 1) < 64
                a, c = jnp.where(low, a, pltpu.roll(c, 64, 1)), jnp.where(low, pltpu.roll(a, 64, 1), c)
            hid[r, tile * 128 : tile * 128 + 128] = gated(a, c)

    starts = [sum(len(g) for g in groups[:i]) for i in range(len(groups))]

    def half(ref, i, h):
        return ref.at[pl.ds(starts[i], len(groups[i])), pl.ds(h * 128, 128), :]

    def x_copy(kind, i, h):
        src, dst, link = {
            ("far", 0): (far_s, far_r, "x+"), ("far", 1): (far_s, far_r, "x-"),
            ("m", 0): (near_m, in_m, "x-"), ("m", 1): (near_p, in_m, "x+"),
            ("n", 0): (near_p, in_n, "x+"), ("n", 1): (near_m, in_n, "x-"),
        }[(kind, h)]
        c = ("far", "m", "n").index(kind)
        return pltpu.make_async_remote_copy(
            src_ref=half(src, i, h), dst_ref=half(dst, i, h), send_sem=send_sem.at[4 + c],
            recv_sem=x_recv.at[(c * 9 + i) * 2 + h], device_id=peers[link], device_id_type=pl.DeviceIdType.MESH)

    def x_wait(kind, i, h):
        dst = {"far": far_r, "m": in_m, "n": in_n}[kind]
        c = ("far", "m", "n").index(kind)
        ref = half(dst, i, h)
        pltpu.make_async_copy(ref, ref, x_recv.at[(c * 9 + i) * 2 + h]).wait()

    def down(i, b):
        need_passed("d", groups[i])

        def part(s):
            w = [(c, lo, hi) for lo, hi in ((0, FM), (FM, F)) for c in range(2)]
            return jnp.concatenate([wdn[shard[s], c, lo:hi, :] for c, lo, hi in w], axis=0)

        right = [part(s) for s in groups[i]]
        right = right[0] if len(right) == 1 else jnp.concatenate(right, axis=1)
        prod = jnp.dot(hid[pl.ds(b * TT, TT), :], right, preferred_element_type=jnp.float32)
        to = (far_s, near_p, near_m, own)[b]
        for j in range(len(groups[i])):
            to[starts[i] + j, :, :] = prod[:, j * 128 : j * 128 + 128].astype(to.dtype)
        if b == 0:
            x_copy("far", i, 0).start()
            x_copy("far", i, 1).start()
        if b == 1:
            x_copy("m", i, 1).start()
        if b == 2:
            x_copy("m", i, 0).start()

    for op, *a in plan:
        if op == "send":
            copy_piece(*a).start()
        elif op == "recv":
            recv_piece(*a)
        elif op == "pass":
            pass_shard(*a)
        elif op == "norm":
            norm(*a)
        elif op == "acc":
            accumulate(*a)
        elif op == "fin":
            finish(*a)
        else:
            down(*a)

    f32 = jnp.float32
    for i in range(len(groups)):
        for h in range(2):
            x_wait("far", i, h)
            ref = (near_p, near_m)[h]
            at = (pl.ds(starts[i], len(groups[i])), pl.ds(h * 128, 128), slice(None))
            ref[at] = (ref[at].astype(f32) + far_r[at].astype(f32)).astype(jnp.bfloat16)
            x_copy("n", i, h).start()
    for i in range(len(groups)):
        for h in range(2):
            x_wait("m", i, h)
            x_wait("n", i, h)
        for j, s in enumerate(groups[i]):
            u = starts[i] + j
            total = own[u] + in_m[u].astype(f32) + in_n[u].astype(f32)
            out_ref[:, pl.ds(pl.multiple_of(shard[s] * 128, 128), 128)] = total.astype(jnp.bfloat16)

    sent = (wgu.at[0, pl.ds(0, 1920), :], wdn.at[pl.ds(0, 15), 0], wgu.at[0], wdn.at[:, 0], far_s, near_p, near_m)
    for i, ref in enumerate(sent):
        pltpu.make_async_copy(ref, ref, send_sem.at[i]).wait()


def per_device(tokens, norm_gain, gate_weight, up_weight, down_weight):
    cols = []
    for lo in range(0, F, 128):
        hi = min(lo + 128, F)
        cols += [gate_weight[:, lo:hi], up_weight[:, lo:hi]]
    gu = jnp.concatenate(cols, axis=1)
    vmem, dma = pltpu.VMEM, pltpu.SemaphoreType.DMA
    bf, f32 = jnp.bfloat16, jnp.float32
    unit = (N_FS, TT, 128)
    any_spec = pl.BlockSpec(memory_space=pl.ANY)
    return pl.pallas_call(
        kernel,
        out_shape=jax.ShapeDtypeStruct((TT, D), bf),
        in_specs=[any_spec, pl.BlockSpec(memory_space=pltpu.VMEM), any_spec, any_spec],
        out_specs=pl.BlockSpec(memory_space=pltpu.VMEM),
        scratch_shapes=[
            vmem((4, TT, D), bf), vmem((N_FS, 4 * TT, 128), bf), vmem((2, D, 2 * F), bf), vmem((N_FS, 2, F, 128), bf),
            vmem((11, 4 * TT, 256), f32), vmem((4 * TT, 2 * F), bf),
            vmem(unit, bf), vmem(unit, bf), vmem(unit, bf), vmem(unit, bf), vmem(unit, bf), vmem(unit, bf), vmem(unit, f32),
            dma((2,)), dma((4,)), dma((64,)), dma((64,)), dma((16,)), dma((16,)), dma((54,)), dma((7,)),
        ],
        compiler_params=pltpu.CompilerParams(collective_id=0, has_side_effects=True, vmem_limit_bytes=63 * 2**20),
        name="ffn",
    )(tokens, norm_gain.reshape(1, D), gu, down_weight)


def solution(mesh):
    placed = (P("fs", None), P(), P("fs", "tp"), P("fs", "tp"), P("tp", "fs"))
    return jax.shard_map(
        per_device, mesh=mesh, in_specs=placed, out_specs=P(("fs", "tp"), None), check_vma=False
    )
```

time: 192 us -> 108 us (0.56); the launches traced: 192 us -> 106 us
  waiting for transfers between devices: 129 us -> 0 us
  Pallas kernels: 0 us -> 98.3 us
  matrix products: 30.5 us -> 0 us
  between operations: 13.4 us -> 0.07 us
  starting transfers between devices: 8.76 us -> 0 us
  other arithmetic: 7.1 us -> 0 us
  local copies, waits for them, and re-layouts: 3.06 us -> 7.7 us
    pallas_call x0 -> x1, Pallas kernels: none -> 98.3 us  [per_device(): pl.pallas_call(kernel, out_shape=jax.ShapeDtypeStruct((TT, D), bf), in_sp...]
    all_gather x1 -> x0, waiting for transfers between devices: 76.7 us -> none  [side_by_side(): whole = lax.all_gather(both, axis, axis=dim, tiled=True)]
    reduce_scatter x1 -> x0, waiting for transfers between devices: 52.6 us -> none  [per_device(): lax.psum_scatter(jnp.dot(hidden, down_full, preferred_element_type=jnp.fl...]
    dot_general x2 -> x0, matrix products: 30.5 us -> none  [the longest x1 19.3 us: per_device(): jnp.dot(hidden, down_full, preferred_element_type=jnp.float32)]
    all_to_all x1 -> x0, starting transfers between devices: 8.72 us -> none  [from_everyone(): return lax.all_to_all(copies, axis, split_axis=0, concat_axis=0, tiled=True)]
    reduce_sum x1 -> x0, other arithmetic: 5.32 us -> none  [per_device(): scale = lax.rsqrt(jnp.mean(xf * xf, axis=-1, keepdims=True) + 1e-06)]
    unnamed x2 -> x13, local copies, waits for them, and re-layouts: 0.01 us -> 3.72 us
    slice x0 -> x4, local copies, waits for them, and re-layouts: none -> 3.14 us  [per_device(): cols += [gate_weight[:, lo:hi], up_weight[:, lo:hi]]]
  transfers between devices with their start and end apart: 3 -> 0, of which waited for: 2 -> 0; matrix products, arithmetic and copies ran while one was open for 10% -> 0% of each run, Pallas kernels for 0% -> 0%
where the time goes in v1:
time: 108 us; the launch traced here: 106 us
  Pallas kernels  98.3 us (91%)
  local copies, waits for them, and re-layouts  7.7 us (7%)
    pallas_call x1, Pallas kernels, per_device(): pl.pallas_call(kernel, out_shape=jax.ShapeDtypeStruct((TT, D), bf), in_sp...  98.3 us
    unnamed x13, local copies, waits for them, and re-layouts  3.72 us
    slice x4, local copies, waits for them, and re-layouts, per_device(): cols += [gate_weight[:, lo:hi], up_weight[:, lo:hi]]  3.14 us

profile of v1, /device:TPU:1, one launch (start us, length us, event | category | flops | bytes accessed | tf_op | source)
XLA Modules:
  0.0 106.1 jit_solution(17038627897873666336)
XLA Ops:
  0.0 0.7 slice.46
  0.7 0.1 copy.28
  0.8 0.7 slice.47
  1.6 0.1 copy.29
  1.7 0.8 fusion.1
  2.5 0.1 copy.26
  2.6 0.1 copy.24
  2.8 0.1 copy.22
  2.9 0.1 copy.20
  3.0 0.1 copy.18
  3.2 0.8 fusion
  4.0 0.1 copy.27
  4.1 0.1 copy.25
  4.2 0.1 copy.23
  4.4 0.1 copy.21
  4.5 0.1 copy.19
  4.6 0.8 concatenate.3.gu_hbm
  5.5 98.3 %ffn.1 = bf16[256,2048]{1,0:T(8,128)(2,1)} custom-call(bf16[2048,2048]{1,0:T(8,128)(2,1)} %tok_hbm.1, f32[1,2048]{1,0:T(1,128)} %bitcast.1, bf16[128,1408]{1,0:T(8,128)(2,1)} %concatenate.3.gu_hbm, bf16[704,128]{1,0:T(8,128)(2,1)} %dn_hbm.1), custom_call_target="tpu_custom_call" | custom-call | tf_op jit(solution)/shard_map/ffn/pallas_call | solution.py:351
  103.8 2.3 %copy.31 = bf16[256,2048]{1,0:T(8,128)(2,1)} copy(bf16[256,2048]{1,0:T(8,128)(2,1)} %ffn.1) | data formatting | bytes 2097152

commit v2 on v1

--- a/solution.py
+++ b/solution.py
@@ -12,8 +12,9 @@
 F = 704
 FM = 640
 TT = 256
-GQ = 32
+GQ = 352
 DQ = 176
+RANK = {1: 1, 2: 2, 4: 3, 5: 4, 8: 5}
 LINKS = ("y+", "y-", "z+", "z-")
 FIRST = {"y+": (0, 1, 2, 3), "y-": (1, 0, 3, 2), "z+": (2, 3, 0, 1), "z-": (3, 2, 1, 0)}
 
@@ -47,14 +48,16 @@
     def offer(l, k, q, dz, dy):
         nonlocal n
         n += 1
-        heapq.heappush(heap[l], (k == "d", n, k, q, dz, dy))
+        tz, ty = seen_from(l, dz, dy)
+        early = tz == 0 if q < 2 else ty == 0
+        heapq.heappush(heap[l], (k == "d", 0 if early else RANK[tz * tz + ty * ty], n, k, q, dz, dy))
 
     def top_up(t):
         nonlocal n
         sends = []
         for l in LINKS:
-            while heap[l] and free[l] - t < backlog and (heap[l][0][2] == "g" or count[l] >= 15):
-                _, _, k, q, dz, dy = heapq.heappop(heap[l])
+            while heap[l] and free[l] - t < backlog and (heap[l][0][0] == 0 or count[l] >= 15):
+                _, _, _, k, q, dz, dy = heapq.heappop(heap[l])
                 count[l] += 1
                 n += 1
                 free[l] = max(t, free[l]) + unit[k]
@@ -75,49 +78,63 @@
     return events
 
 
-def make_plan(unit={"g": 1.93, "d": 0.97}, lat=2.0, backlog=6.0, sib=1.8):
+def make_plan(unit={"g": 1.93, "d": 0.97}, lat=2.2, backlog=6.0, sib=1.8, sizes=(5, 6, 2, 3), margin=0.4, log=None):
     events = gather_events(unit, lat, backlog)
     done, left = {("g", 0, 0): 0.0, ("d", 0, 0): 0.0}, {}
     for t, what, _ in events[1:]:
         k, q, dz, dy = what
         left[(k, dz, dy)] = left.get((k, dz, dy), 0) + 1
         if left[(k, dz, dy)] == 4:
-            done[(k, dz, dy)] = t
+            done[(k, dz, dy)] = t + margin
     order = {k: [key[1:] for key in sorted((key for key in done if key[0] == k), key=lambda key: done[key])] for k in "gd"}
     assert len(order["g"]) == 16 and len(order["d"]) == 16
-    steps = [order["g"][4 * i : 4 * i + 4] for i in range(4)]
+    steps = [order["g"][sum(sizes[:i]) : sum(sizes[: i + 1])] for i in range(len(sizes))]
     groups = [order["d"][:1]] + [order["d"][1 + 2 * i : 3 + 2 * i] for i in range(7)] + [order["d"][15:]]
-    work = [(1.5, 1.2, ("norm", b)) for b in range(4)]
-    for i in range(3):
+    last = len(steps) - 1
+    work = [(0.0, 1.9, ("norm", b)) for b in range(4)]
+    for i in range(last):
         ready = max(done[("g", *s)] for s in steps[i])
-        work.append((ready, 2.2, ("acc", i, 0)))
-        work.append((ready + sib, 2.2, ("acc", i, 1)))
-        work.append((ready + sib, 0.5, ("acc", i, 2)))
-    ready = max(done[("g", *s)] for s in steps[3]) + sib
+        cost = 0.43 * len(steps[i])
+        work.append((ready, cost, ("acc", i, 0)))
+        work.append((ready + sib, cost, ("acc", i, 1)))
+        work.append((ready + sib, cost * 0.35, ("acc", i, 2)))
+    cost = 0.45 + 0.15 * len(steps[last])
+    ready = max(done[("g", *s)] for s in steps[last]) + sib
     for b in range(4):
-        work += [(ready, 1.2, ("fin", b)), (ready, 0.3, ("down", 0, b))]
+        work += [(ready, cost, ("fin", b)), (ready, 0.38, ("down", 0, b))]
     for i in range(1, len(groups)):
         ready = max(done[("d", *s)] for s in groups[i]) + sib
-        work += [(ready, 0.4, ("down", i, b)) for b in range(4)]
-    plan, now, w, got = [], 0.0, 0, {}
-    plan += [("send", *s) for s in events[0][2]] + [("pass", "g", 0, 0), ("pass", "d", 0, 0)]
-    for t, what, sends in events[1:]:
-        while w < len(work) and max(now, work[w][0]) + work[w][1] <= t + 0.6:
-            plan.append(work[w][2])
-            now = max(now, work[w][0]) + work[w][1]
-            w += 1
-        k, q, dz, dy = what
-        plan.append(("recv", *what))
-        now = max(now, t)
-        plan += [("send", *s) for s in sends]
-        got[(k, dz, dy)] = got.get((k, dz, dy), 0) + 1
-        if got[(k, dz, dy)] == 4:
-            plan.append(("pass", k, dz, dy))
-    plan += [item[2] for item in work[w:]]
+        if i == 1:
+            work += [(ready, 0.55, ("down", i, b)) for b in range(4)]
+        else:
+            work.append((ready, 1.8, ("down", i, None)))
+        if i == 2:
+            work.append((ready, 0.1, ("add", 0)))
+    work += [(0.0, 0.1, ("add", i)) for i in range(1, len(groups))]
+    plan, now, got, events = [], 0.0, {}, events[::-1]
+    plan += [("send", *s) for s in events.pop()[2]] + [("pass", "g", 0, 0), ("pass", "d", 0, 0)]
+    work = work[::-1]
+    while events or work:
+        if events and (not work or events[-1][0] + margin <= max(now, work[-1][0])):
+            t, what, sends = events.pop()
+            k, q, dz, dy = what
+            plan.append(("recv", *what))
+            now = max(now, t + margin)
+            plan += [("send", *s) for s in sends]
+            got[(k, dz, dy)] = got.get((k, dz, dy), 0) + 1
+            if got[(k, dz, dy)] == 4:
+                plan.append(("pass", k, dz, dy))
+        else:
+            ready, cost, op = work.pop()
+            now = max(now, ready)
+            plan.append(op)
+            if log is not None:
+                log.append((round(now, 1), op))
+            now += cost
     return plan, steps, groups
 
 
-def kernel(tok_hbm, gain_ref, gu_hbm, dn_hbm, out_ref, tok, normed, wgu, wdn, acc, hid, far_s, far_r, near_p, near_m,
+def kernel(tok_hbm, gain_ref, gate_hbm, up_hbm, dn_hbm, out_ref, tok, normed, wgu, wdn, acc, hid, far_s, far_r, near_p, near_m,
            in_m, in_n, own, loc_sem, tok_sem, g_recv, d_recv, gs_recv, ds_recv, x_recv, send_sem):
     plan, steps, groups = make_plan()
     fs, tp = lax.axis_index("fs"), lax.axis_index("tp")
@@ -140,12 +157,9 @@
     def label(dz, dy):
         return (dz + 1) * 4 + dy + 1
 
-    def rows(dz, dy, at, size):
-        return pl.ds(pl.multiple_of(shard[(dz, dy)] * 128 + at, size), size)
-
     def piece(k, q, dz, dy):
         if k == "g":
-            return wgu.at[0, rows(dz, dy, q * GQ, GQ), :]
+            return wgu.at[shard[(dz, dy)], 0, pl.ds(q * GQ, GQ), :]
         return wdn.at[shard[(dz, dy)], 0, pl.ds(q * DQ, DQ), :]
 
     def copy_piece(link, k, q, dz, dy):
@@ -162,9 +176,7 @@
         pltpu.make_async_copy(ref, ref, sem).wait()
 
     def whole(k, slot, dz, dy):
-        if k == "g":
-            return wgu.at[slot, rows(dz, dy, 0, 128), :]
-        return wdn.at[shard[(dz, dy)], slot]
+        return (wgu if k == "g" else wdn).at[shard[(dz, dy)], slot]
 
     def pass_shard(k, dz, dy):
         sems, s = (gs_recv, 2) if k == "g" else (ds_recv, 3)
@@ -181,9 +193,14 @@
                 ref = whole(k, 1, *s)
                 pltpu.make_async_copy(ref, ref, (gs_recv if k == "g" else ds_recv).at[label(*s)]).wait()
 
-    own_g = pltpu.make_async_copy(gu_hbm, whole("g", 0, 0, 0), loc_sem.at[0])
-    own_d = pltpu.make_async_copy(dn_hbm, whole("d", 0, 0, 0), loc_sem.at[1])
+    barrier = pltpu.get_barrier_semaphore()
+    for peer in peers.values():
+        pl.semaphore_signal(barrier, inc=1, device_id=peer, device_id_type=pl.DeviceIdType.MESH)
+    own_g = pltpu.make_async_copy(gate_hbm, whole("g", 0, 0, 0).at[pl.ds(0, F), :], loc_sem.at[0])
+    own_u = pltpu.make_async_copy(up_hbm, whole("g", 0, 0, 0).at[pl.ds(F, F), :], loc_sem.at[1])
+    own_d = pltpu.make_async_copy(dn_hbm, whole("d", 0, 0, 0), loc_sem.at[2])
     own_g.start()
+    own_u.start()
     own_d.start()
 
     def tok_copy(b):
@@ -191,15 +208,12 @@
         at = pl.multiple_of((to * 2 + core) * TT, TT)
         return pltpu.make_async_copy(tok_hbm.at[pl.ds(at, TT), :], tok.at[b], tok_sem.at[b])
 
+    own_g.wait()
+    own_u.wait()
+    own_d.wait()
     for b in range(4):
         tok_copy(b).start()
-
-    barrier = pltpu.get_barrier_semaphore()
-    for peer in peers.values():
-        pl.semaphore_signal(barrier, inc=1, device_id=peer, device_id_type=pl.DeviceIdType.MESH)
     pl.semaphore_wait(barrier, len(peers))
-    own_g.wait()
-    own_d.wait()
 
     def norm(b):
         tok_copy(b).wait()
@@ -217,13 +231,18 @@
     def lhs(step, r):
         return jnp.concatenate([normed[shard[s], r, :] for s in step], axis=1)
 
-    def rhs(step, tile):
+    def times(left, step, tile):
         def part(s):
+            at = shard[s]
             if tile < 10:
-                return wgu[tile // 5, rows(*s, 0, 128), (tile % 5) * 256 : (tile % 5) * 256 + 256]
-            return jnp.concatenate([wgu[c, rows(*s, 0, 128), 2 * FM : 2 * F] for c in range(2)], axis=1)
-
-        return jnp.concatenate([part(s) for s in step], axis=0)
+                lo = (tile % 5) * 128
+                cuts = [(tile // 5, lo, lo + 128), (tile // 5, F + lo, F + lo + 128)]
+            else:
+                cuts = [(c, lo, lo + F - FM) for lo in (FM, F + FM) for c in range(2)]
+            return jnp.concatenate([wgu[at, c, lo:hi, :] for c, lo, hi in cuts], axis=0)
+
+        right = jnp.concatenate([part(s) for s in step], axis=1)
+        return lax.dot_general(left, right, (((1,), (1,)), ((), ())), preferred_element_type=jnp.float32)
 
     def accumulate(i, part):
         step = steps[i]
@@ -236,7 +255,7 @@
             r = pl.ds(pl.multiple_of(h * 512, 512), 512)
             left = lhs(step, r)
             for tile in tiles:
-                prod = jnp.dot(left, rhs(step, tile), preferred_element_type=jnp.float32)
+                prod = times(left, step, tile)
                 if i == 0:
                     acc[tile, r, :] = prod
                 else:
@@ -246,15 +265,12 @@
         return (g / (1.0 + jnp.exp(-g)) * u).astype(jnp.bfloat16)
 
     def finish(b):
-        need_passed("g", steps[3])
+        need_passed("g", steps[-1])
         r = pl.ds(b * TT, TT)
-        left = lhs(steps[3], r)
+        left = lhs(steps[-1], r)
         for tile in range(11):
-            v = acc[tile, r, :] + jnp.dot(left, rhs(steps[3], tile), preferred_element_type=jnp.float32)
+            v = acc[tile, r, :] + times(left, steps[-1], tile)
             a, c = v[:, :128], v[:, 128:]
-            if tile == 10:
-                low = lax.broadcasted_iota(jnp.int32, a.shape, 1) < 64
-                a, c = jnp.where(low, a, pltpu.roll(c, 64, 1)), jnp.where(low, pltpu.roll(a, 64, 1), c)
             hid[r, tile * 128 : tile * 128 + 128] = gated(a, c)
 
     starts = [sum(len(g) for g in groups[:i]) for i in range(len(groups))]
@@ -288,17 +304,23 @@
 
         right = [part(s) for s in groups[i]]
         right = right[0] if len(right) == 1 else jnp.concatenate(right, axis=1)
-        prod = jnp.dot(hid[pl.ds(b * TT, TT), :], right, preferred_element_type=jnp.float32)
-        to = (far_s, near_p, near_m, own)[b]
-        for j in range(len(groups[i])):
-            to[starts[i] + j, :, :] = prod[:, j * 128 : j * 128 + 128].astype(to.dtype)
-        if b == 0:
-            x_copy("far", i, 0).start()
-            x_copy("far", i, 1).start()
-        if b == 1:
-            x_copy("m", i, 1).start()
-        if b == 2:
-            x_copy("m", i, 0).start()
+        blocks = range(4) if b is None else (b,)
+        r = slice(None) if b is None else pl.ds(b * TT, TT)
+        prod = jnp.dot(hid[r, :], right, preferred_element_type=jnp.float32)
+        for n, blk in enumerate(blocks):
+            to = (far_s, near_p, near_m, own)[blk]
+            for j in range(len(groups[i])):
+                to[starts[i] + j, :, :] = prod[n * TT : n * TT + TT, j * 128 : j * 128 + 128].astype(to.dtype)
+            for kind, h in ((("far", 0), ("far", 1)), (("m", 1),), (("m", 0),), ())[blk]:
+                x_copy(kind, i, h).start()
+
+    def add_far(i):
+        for h in range(2):
+            x_wait("far", i, h)
+            ref = (near_p, near_m)[h]
+            at = (pl.ds(starts[i], len(groups[i])), pl.ds(h * 128, 128), slice(None))
+            ref[at] = (ref[at].astype(jnp.float32) + far_r[at].astype(jnp.float32)).astype(jnp.bfloat16)
+            x_copy("n", i, h).start()
 
     for op, *a in plan:
         if op == "send":
@@ -313,17 +335,12 @@
             accumulate(*a)
         elif op == "fin":
             finish(*a)
+        elif op == "add":
+            add_far(*a)
         else:
             down(*a)
 
     f32 = jnp.float32
-    for i in range(len(groups)):
-        for h in range(2):
-            x_wait("far", i, h)
-            ref = (near_p, near_m)[h]
-            at = (pl.ds(starts[i], len(groups[i])), pl.ds(h * 128, 128), slice(None))
-            ref[at] = (ref[at].astype(f32) + far_r[at].astype(f32)).astype(jnp.bfloat16)
-            x_copy("n", i, h).start()
     for i in range(len(groups)):
         for h in range(2):
             x_wait("m", i, h)
@@ -333,35 +350,31 @@
             total = own[u] + in_m[u].astype(f32) + in_n[u].astype(f32)
             out_ref[:, pl.ds(pl.multiple_of(shard[s] * 128, 128), 128)] = total.astype(jnp.bfloat16)
 
-    sent = (wgu.at[0, pl.ds(0, 1920), :], wdn.at[pl.ds(0, 15), 0], wgu.at[0], wdn.at[:, 0], far_s, near_p, near_m)
+    sent = (wgu.at[pl.ds(0, 15), 0], wdn.at[pl.ds(0, 15), 0], wgu.at[:, 0], wdn.at[:, 0], far_s, near_p, near_m)
     for i, ref in enumerate(sent):
         pltpu.make_async_copy(ref, ref, send_sem.at[i]).wait()
 
 
 def per_device(tokens, norm_gain, gate_weight, up_weight, down_weight):
-    cols = []
-    for lo in range(0, F, 128):
-        hi = min(lo + 128, F)
-        cols += [gate_weight[:, lo:hi], up_weight[:, lo:hi]]
-    gu = jnp.concatenate(cols, axis=1)
     vmem, dma = pltpu.VMEM, pltpu.SemaphoreType.DMA
     bf, f32 = jnp.bfloat16, jnp.float32
     unit = (N_FS, TT, 128)
-    any_spec = pl.BlockSpec(memory_space=pl.ANY)
+    args = (tokens, norm_gain.reshape(1, D), gate_weight.T, up_weight.T, down_weight)
+    any_spec = pl.BlockSpec(memory_space=pltpu.HBM)
     return pl.pallas_call(
         kernel,
         out_shape=jax.ShapeDtypeStruct((TT, D), bf),
-        in_specs=[any_spec, pl.BlockSpec(memory_space=pltpu.VMEM), any_spec, any_spec],
+        in_specs=[any_spec, pl.BlockSpec(memory_space=pltpu.VMEM), any_spec, any_spec, any_spec],
         out_specs=pl.BlockSpec(memory_space=pltpu.VMEM),
         scratch_shapes=[
-            vmem((4, TT, D), bf), vmem((N_FS, 4 * TT, 128), bf), vmem((2, D, 2 * F), bf), vmem((N_FS, 2, F, 128), bf),
+            vmem((4, TT, D), bf), vmem((N_FS, 4 * TT, 128), bf), vmem((N_FS, 2, 2 * F, 128), bf), vmem((N_FS, 2, F, 128), bf),
             vmem((11, 4 * TT, 256), f32), vmem((4 * TT, 2 * F), bf),
             vmem(unit, bf), vmem(unit, bf), vmem(unit, bf), vmem(unit, bf), vmem(unit, bf), vmem(unit, bf), vmem(unit, f32),
-            dma((2,)), dma((4,)), dma((64,)), dma((64,)), dma((16,)), dma((16,)), dma((54,)), dma((7,)),
+            dma((3,)), dma((4,)), dma((64,)), dma((64,)), dma((16,)), dma((16,)), dma((54,)), dma((7,)),
         ],
-        compiler_params=pltpu.CompilerParams(collective_id=0, has_side_effects=True, vmem_limit_bytes=63 * 2**20),
+        compiler_params=pltpu.CompilerParams(collective_id=0, has_side_effects=True, vmem_limit_bytes=52 * 2**20),
         name="ffn",
-    )(tokens, norm_gain.reshape(1, D), gu, down_weight)
+    )(*(pltpu.with_memory_space_constraint(a, pltpu.HBM) for a in args))
 
 
 def solution(mesh):

time: 108 us -> 86.1 us (0.80); the launches traced: 106 us -> 85.9 us
  Pallas kernels: 98.3 us -> 84.9 us
  local copies, waits for them, and re-layouts: 7.7 us -> 0.97 us
    pallas_call x1, Pallas kernels: 98.3 us -> 84.9 us  [per_device(): pl.pallas_call(kernel, out_shape=jax.ShapeDtypeStruct((TT, D), bf), in_sp...]
    slice x4 -> x0, local copies, waits for them, and re-layouts: 3.14 us -> none  [per_device(): cols += [gate_weight[:, lo:hi], up_weight[:, lo:hi]]]
    unnamed x13 -> x1, local copies, waits for them, and re-layouts: 3.72 us -> 0.97 us
where the time goes in v2:
time: 86.1 us; the launch traced here: 85.9 us
  Pallas kernels  84.9 us (99%)
  local copies, waits for them, and re-layouts  0.97 us (1%)
    pallas_call x1, Pallas kernels, per_device(): pl.pallas_call(kernel, out_shape=jax.ShapeDtypeStruct((TT, D), bf), in_sp...  84.9 us

profile of v2, /device:TPU:1, one launch (start us, length us, event | category | flops | bytes accessed | tf_op | source)
XLA Modules:
  0.0 85.9 jit_solution(1467800512031491802)
XLA Ops:
  0.0 84.9 %ffn.1 = bf16[256,2048]{1,0:T(8,128)(2,1)S(1)} custom-call(bf16[2048,2048]{1,0:T(8,128)(2,1)} %tok_hbm.1, f32[1,2048]{1,0:T(1,128)} %bitcast.5, bf16[704,128]{1,0:T(8,128)(2,1)} %bitcast.3, bf16[704,128]{1,0:T(8,128)(2,1)} %bitcast.4, bf16[704,128]{1,0:T(8,128)(2,1)} %dn_hbm.1), custom_call_target="tpu_custom_call" | custom-call | tf_op jit(solution)/shard_map/ffn/pallas_call | solution.py:364
  84.9 1.0 %copy.7 = bf16[256,2048]{1,0:T(8,128)(2,1)} copy(bf16[256,2048]{1,0:T(8,128)(2,1)S(1)} %ffn.1) | data formatting | bytes 2097152

commit v3 on v2

--- a/solution.py
+++ b/solution.py
@@ -37,6 +37,12 @@
 def seen_from(link, dz, dy):
     step = 1 if link[1] == "+" else -1
     return (near(dz - step), dy) if link[0] == "z" else (dz, near(dy - step))
+
+
+def turn(q, dz, dy):
+    a, b = (dy, dz) if q < 2 else (dz, dy)
+    sign = 1 - 2 * (q % 2)
+    return (near(sign * a) + 1) * 4 + near(sign * b) + 1
 
 
 def gather_events(unit, lat, backlog):
@@ -70,11 +76,17 @@
             for q in FIRST[l]:
                 offer(l, k, q, 0, 0)
     events = [(0.0, None, top_up(0.0))]
+    here = {}
     while flying:
         t, _, k, q, dz, dy = heapq.heappop(flying)
-        for l in onward(q, dz, dy):
-            offer(l, k, q, dz, dy)
-        events.append((t, (k, q, dz, dy), top_up(t)))
+        some = here.setdefault((k, turn(q, dz, dy)), [])
+        some.append((q, dz, dy))
+        if len(some) == 4:
+            for piece in some:
+                for l in onward(*piece):
+                    offer(l, k, *piece)
+            events.append((t, (k, turn(q, dz, dy), some), top_up(t)))
+    assert len(events) == 31
     return events
 
 
@@ -82,10 +94,11 @@
     events = gather_events(unit, lat, backlog)
     done, left = {("g", 0, 0): 0.0, ("d", 0, 0): 0.0}, {}
     for t, what, _ in events[1:]:
-        k, q, dz, dy = what
-        left[(k, dz, dy)] = left.get((k, dz, dy), 0) + 1
-        if left[(k, dz, dy)] == 4:
-            done[(k, dz, dy)] = t + margin
+        for _, dz, dy in what[2]:
+            key = (what[0], dz, dy)
+            left[key] = left.get(key, 0) + 1
+            if left[key] == 4:
+                done[key] = t + margin
     order = {k: [key[1:] for key in sorted((key for key in done if key[0] == k), key=lambda key: done[key])] for k in "gd"}
     assert len(order["g"]) == 16 and len(order["d"]) == 16
     steps = [order["g"][sum(sizes[:i]) : sum(sizes[: i + 1])] for i in range(len(sizes))]
@@ -99,43 +112,45 @@
         work.append((ready + sib, cost, ("acc", i, 1)))
         work.append((ready + sib, cost * 0.35, ("acc", i, 2)))
     cost = 0.45 + 0.15 * len(steps[last])
-    ready = max(done[("g", *s)] for s in steps[last]) + sib
+    ready = max(done[("g", *s)] for s in steps[last])
+    late = max(done[("d", *s)] for s in groups[1]) + sib
     for b in range(4):
         work += [(ready, cost, ("fin", b)), (ready, 0.38, ("down", 0, b))]
-    for i in range(1, len(groups)):
+    work[-1:] = [(late, 0.55, ("down", 1, b)) for b in range(3)] + work[-1:] + [(late, 0.55, ("down", 1, 3))]
+    for i in range(2, len(groups)):
         ready = max(done[("d", *s)] for s in groups[i]) + sib
-        if i == 1:
-            work += [(ready, 0.55, ("down", i, b)) for b in range(4)]
-        else:
-            work.append((ready, 1.8, ("down", i, None)))
+        work.append((ready, 1.8, ("down", i, None)))
         if i == 2:
             work.append((ready, 0.1, ("add", 0)))
-    work += [(0.0, 0.1, ("add", i)) for i in range(1, len(groups))]
+    work += [(60.0, 0.1, ("add", i)) for i in range(1, len(groups))]
     plan, now, got, events = [], 0.0, {}, events[::-1]
     plan += [("send", *s) for s in events.pop()[2]] + [("pass", "g", 0, 0), ("pass", "d", 0, 0)]
-    work = work[::-1]
     while events or work:
-        if events and (not work or events[-1][0] + margin <= max(now, work[-1][0])):
+        free = [item for item in work if item[0] <= now]
+        soon = min([item[0] for item in work], default=1e9)
+        if events and events[-1][0] + margin <= (now if free else soon):
             t, what, sends = events.pop()
-            k, q, dz, dy = what
-            plan.append(("recv", *what))
+            plan.append(("recv", *what[:2]))
             now = max(now, t + margin)
             plan += [("send", *s) for s in sends]
-            got[(k, dz, dy)] = got.get((k, dz, dy), 0) + 1
-            if got[(k, dz, dy)] == 4:
-                plan.append(("pass", k, dz, dy))
+            for _, dz, dy in what[2]:
+                key = (what[0], dz, dy)
+                got[key] = got.get(key, 0) + 1
+                if got[key] == 4:
+                    plan.append(("pass", *key))
+        elif free:
+            work.remove(free[0])
+            plan.append(free[0][2])
+            if log is not None:
+                log.append((round(now, 1), free[0][2]))
+            now += free[0][1]
         else:
-            ready, cost, op = work.pop()
-            now = max(now, ready)
-            plan.append(op)
-            if log is not None:
-                log.append((round(now, 1), op))
-            now += cost
+            now = soon
     return plan, steps, groups
 
 
-def kernel(tok_hbm, gain_ref, gate_hbm, up_hbm, dn_hbm, out_ref, tok, normed, wgu, wdn, acc, hid, far_s, far_r, near_p, near_m,
-           in_m, in_n, own, loc_sem, tok_sem, g_recv, d_recv, gs_recv, ds_recv, x_recv, send_sem):
+def kernel(tok_hbm, gain_hbm, gate_hbm, up_hbm, dn_hbm, out_ref, tok, normed, wgu, wdn, acc, hid, far_s, far_r, near_p, near_m,
+           come, own, loc_sem, tok_sem, g_recv, d_recv, gs_recv, ds_recv, x_recv, send_sem, gain_ref):
     plan, steps, groups = make_plan()
     fs, tp = lax.axis_index("fs"), lax.axis_index("tp")
     z, y = fs // 4, fs % 4
@@ -154,9 +169,6 @@
     peers = {l: dev(l) for l in LINKS + ("x+", "x-", "c+")}
     shard = {(dz, dy): ((z + dz + 4) % 4) * 4 + (y + dy + 4) % 4 for dz in range(-1, 3) for dy in range(-1, 3)}
 
-    def label(dz, dy):
-        return (dz + 1) * 4 + dy + 1
-
     def piece(k, q, dz, dy):
         if k == "g":
             return wgu.at[shard[(dz, dy)], 0, pl.ds(q * GQ, GQ), :]
@@ -167,31 +179,33 @@
         ref = piece(k, q, dz, dy)
         sems, s = (g_recv, 0) if k == "g" else (d_recv, 1)
         return pltpu.make_async_remote_copy(
-            src_ref=ref, dst_ref=ref, send_sem=send_sem.at[s], recv_sem=sems.at[q * 16 + label(*there)],
+            src_ref=ref, dst_ref=ref, send_sem=send_sem.at[s], recv_sem=sems.at[turn(q, *there)],
             device_id=peers[link], device_id_type=pl.DeviceIdType.MESH)
 
-    def recv_piece(k, q, dz, dy):
-        ref = piece(k, q, dz, dy)
-        sem = (g_recv if k == "g" else d_recv).at[q * 16 + label(dz, dy)]
-        pltpu.make_async_copy(ref, ref, sem).wait()
+    def recv_turn(k, at):
+        ref = (wgu if k == "g" else wdn).at[0, 0]
+        pltpu.make_async_copy(ref, ref, (g_recv if k == "g" else d_recv).at[at]).wait()
 
     def whole(k, slot, dz, dy):
         return (wgu if k == "g" else wdn).at[shard[(dz, dy)], slot]
+
+    def batch(k, s):
+        return next(i for i, part in enumerate(steps if k == "g" else groups) if s in part)
 
     def pass_shard(k, dz, dy):
         sems, s = (gs_recv, 2) if k == "g" else (ds_recv, 3)
         pltpu.make_async_remote_copy(
             src_ref=whole(k, 0, dz, dy), dst_ref=whole(k, 1, dz, dy), send_sem=send_sem.at[s],
-            recv_sem=sems.at[label(dz, dy)], device_id=peers["c+"], device_id_type=pl.DeviceIdType.MESH).start()
+            recv_sem=sems.at[batch(k, (dz, dy))], device_id=peers["c+"], device_id_type=pl.DeviceIdType.MESH).start()
 
     passed = set()
 
     def need_passed(k, shards):
-        for s in shards:
-            if (k, *s) not in passed:
-                passed.add((k, *s))
-                ref = whole(k, 1, *s)
-                pltpu.make_async_copy(ref, ref, (gs_recv if k == "g" else ds_recv).at[label(*s)]).wait()
+        at = batch(k, shards[0])
+        if (k, at) not in passed:
+            passed.add((k, at))
+            ref = (wgu if k == "g" else wdn).at[pl.ds(0, len(shards)), 1]
+            pltpu.make_async_copy(ref, ref, (gs_recv if k == "g" else ds_recv).at[at]).wait()
 
     barrier = pltpu.get_barrier_semaphore()
     for peer in peers.values():
@@ -202,6 +216,8 @@
     own_g.start()
     own_u.start()
     own_d.start()
+    gain = pltpu.make_async_copy(gain_hbm, gain_ref, loc_sem.at[3])
+    gain.start()
 
     def tok_copy(b):
         to = (x + (2, 1, 3, 0)[b]) % 4
@@ -211,6 +227,7 @@
     own_g.wait()
     own_u.wait()
     own_d.wait()
+    gain.wait()
     for b in range(4):
         tok_copy(b).start()
     pl.semaphore_wait(barrier, len(peers))
@@ -265,10 +282,11 @@
         return (g / (1.0 + jnp.exp(-g)) * u).astype(jnp.bfloat16)
 
     def finish(b):
-        need_passed("g", steps[-1])
         r = pl.ds(b * TT, TT)
         left = lhs(steps[-1], r)
         for tile in range(11):
+            if tile == 5:
+                need_passed("g", steps[-1])
             v = acc[tile, r, :] + times(left, steps[-1], tile)
             a, c = v[:, :128], v[:, 128:]
             hid[r, tile * 128 : tile * 128 + 128] = gated(a, c)
@@ -281,19 +299,16 @@
     def x_copy(kind, i, h):
         src, dst, link = {
             ("far", 0): (far_s, far_r, "x+"), ("far", 1): (far_s, far_r, "x-"),
-            ("m", 0): (near_m, in_m, "x-"), ("m", 1): (near_p, in_m, "x+"),
-            ("n", 0): (near_p, in_n, "x+"), ("n", 1): (near_m, in_n, "x-"),
+            ("m", 0): (near_m, come.at[0], "x-"), ("m", 1): (near_p, come.at[0], "x+"),
+            ("n", 0): (near_p, come.at[1], "x+"), ("n", 1): (near_m, come.at[1], "x-"),
         }[(kind, h)]
         c = ("far", "m", "n").index(kind)
         return pltpu.make_async_remote_copy(
             src_ref=half(src, i, h), dst_ref=half(dst, i, h), send_sem=send_sem.at[4 + c],
-            recv_sem=x_recv.at[(c * 9 + i) * 2 + h], device_id=peers[link], device_id_type=pl.DeviceIdType.MESH)
-
-    def x_wait(kind, i, h):
-        dst = {"far": far_r, "m": in_m, "n": in_n}[kind]
-        c = ("far", "m", "n").index(kind)
-        ref = half(dst, i, h)
-        pltpu.make_async_copy(ref, ref, x_recv.at[(c * 9 + i) * 2 + h]).wait()
+            recv_sem=x_recv.at[i if kind == "far" else 9 + i], device_id=peers[link], device_id_type=pl.DeviceIdType.MESH)
+
+    def x_wait(ref, i, at):
+        pltpu.make_async_copy(ref, ref, x_recv.at[at]).wait()
 
     def down(i, b):
         need_passed("d", groups[i])
@@ -315,10 +330,11 @@
                 x_copy(kind, i, h).start()
 
     def add_far(i):
+        units = pl.ds(starts[i], len(groups[i]))
+        x_wait(far_r.at[units], i, i)
         for h in range(2):
-            x_wait("far", i, h)
             ref = (near_p, near_m)[h]
-            at = (pl.ds(starts[i], len(groups[i])), pl.ds(h * 128, 128), slice(None))
+            at = (units, pl.ds(h * 128, 128), slice(None))
             ref[at] = (ref[at].astype(jnp.float32) + far_r[at].astype(jnp.float32)).astype(jnp.bfloat16)
             x_copy("n", i, h).start()
 
@@ -326,7 +342,7 @@
         if op == "send":
             copy_piece(*a).start()
         elif op == "recv":
-            recv_piece(*a)
+            recv_turn(*a)
         elif op == "pass":
             pass_shard(*a)
         elif op == "norm":
@@ -342,13 +358,12 @@
 
     f32 = jnp.float32
     for i in range(len(groups)):
-        for h in range(2):
-            x_wait("m", i, h)
-            x_wait("n", i, h)
+        x_wait(come.at[:, pl.ds(starts[i], len(groups[i]))], i, 9 + i)
         for j, s in enumerate(groups[i]):
             u = starts[i] + j
-            total = own[u] + in_m[u].astype(f32) + in_n[u].astype(f32)
-            out_ref[:, pl.ds(pl.multiple_of(shard[s] * 128, 128), 128)] = total.astype(jnp.bfloat16)
+            cols = pl.ds(pl.multiple_of(shard[s] * 128, 128), 128)
+            total = own[u] + come[0, u].astype(f32) + come[1, u].astype(f32)
+            out_ref[:, cols] = total.astype(jnp.bfloat16)
 
     sent = (wgu.at[pl.ds(0, 15), 0], wdn.at[pl.ds(0, 15), 0], wgu.at[:, 0], wdn.at[:, 0], far_s, near_p, near_m)
     for i, ref in enumerate(sent):
@@ -364,13 +379,13 @@
     return pl.pallas_call(
         kernel,
         out_shape=jax.ShapeDtypeStruct((TT, D), bf),
-        in_specs=[any_spec, pl.BlockSpec(memory_space=pltpu.VMEM), any_spec, any_spec, any_spec],
+        in_specs=[any_spec] * 5,
         out_specs=pl.BlockSpec(memory_space=pltpu.VMEM),
         scratch_shapes=[
             vmem((4, TT, D), bf), vmem((N_FS, 4 * TT, 128), bf), vmem((N_FS, 2, 2 * F, 128), bf), vmem((N_FS, 2, F, 128), bf),
             vmem((11, 4 * TT, 256), f32), vmem((4 * TT, 2 * F), bf),
-            vmem(unit, bf), vmem(unit, bf), vmem(unit, bf), vmem(unit, bf), vmem(unit, bf), vmem(unit, bf), vmem(unit, f32),
-            dma((3,)), dma((4,)), dma((64,)), dma((64,)), dma((16,)), dma((16,)), dma((54,)), dma((7,)),
+            vmem(unit, bf), vmem(unit, bf), vmem(unit, bf), vmem(unit, bf), vmem((2, *unit), bf), vmem(unit, f32),
+            dma((4,)), dma((4,)), dma((16,)), dma((16,)), dma((4,)), dma((9,)), dma((18,)), dma((7,)), vmem((1, D), f32),
         ],
         compiler_params=pltpu.CompilerParams(collective_id=0, has_side_effects=True, vmem_limit_bytes=52 * 2**20),
         name="ffn",

time: 86.1 us -> 83.3 us (0.967)
  Pallas kernels: 84.9 us -> 82.2 us
    pallas_call x1, Pallas kernels: 84.9 us -> 82.2 us  [per_device(): pl.pallas_call(kernel, out_shape=jax.ShapeDtypeStruct((TT, D), bf), in_sp...]
where the time goes in v3:
time: 83.3 us; the launch traced here: 83.1 us
  Pallas kernels  82.2 us (99%)
  local copies, waits for them, and re-layouts  0.97 us (1%)
    pallas_call x1, Pallas kernels, per_device(): pl.pallas_call(kernel, out_shape=jax.ShapeDtypeStruct((TT, D), bf), in_sp...  82.2 us

profile of v3, /device:TPU:1, one launch (start us, length us, event | category | flops | bytes accessed | tf_op | source)
XLA Modules:
  0.0 83.1 jit_solution(14179187719445915210)
XLA Ops:
  0.0 82.2 %ffn.1 = bf16[256,2048]{1,0:T(8,128)(2,1)S(1)} custom-call(bf16[2048,2048]{1,0:T(8,128)(2,1)} %tok_hbm.1, f32[1,2048]{1,0:T(1,128)} %bitcast.5, bf16[704,128]{1,0:T(8,128)(2,1)} %bitcast.3, bf16[704,128]{1,0:T(8,128)(2,1)} %bitcast.4, bf16[704,128]{1,0:T(8,128)(2,1)} %dn_hbm.1), custom_call_target="tpu_custom_call" | custom-call | tf_op jit(solution)/shard_map/ffn/pallas_call | solution.py:379
  82.2 1.0 %copy.7 = bf16[256,2048]{1,0:T(8,128)(2,1)} copy(bf16[256,2048]{1,0:T(8,128)(2,1)S(1)} %ffn.1) | data formatting | bytes 2097152

commit v4 on v3

--- a/solution.py
+++ b/solution.py
@@ -90,7 +90,7 @@
     return events
 
 
-def make_plan(unit={"g": 1.93, "d": 0.97}, lat=2.2, backlog=6.0, sib=1.8, sizes=(5, 6, 2, 3), margin=0.4, log=None):
+def make_plan(unit={"g": 1.93, "d": 0.97}, lat=2.2, backlog=6.0, sib=1.8, sizes=(5, 6, 2, 3), margin=0.4, ahead=1.2, log=None):
     events = gather_events(unit, lat, backlog)
     done, left = {("g", 0, 0): 0.0, ("d", 0, 0): 0.0}, {}
     for t, what, _ in events[1:]:
@@ -113,7 +113,7 @@
         work.append((ready + sib, cost * 0.35, ("acc", i, 2)))
     cost = 0.45 + 0.15 * len(steps[last])
     ready = max(done[("g", *s)] for s in steps[last])
-    late = max(done[("d", *s)] for s in groups[1]) + sib
+    late = max(done[("d", *s)] for s in groups[1]) + 0.3
     for b in range(4):
         work += [(ready, cost, ("fin", b)), (ready, 0.38, ("down", 0, b))]
     work[-1:] = [(late, 0.55, ("down", 1, b)) for b in range(3)] + work[-1:] + [(late, 0.55, ("down", 1, 3))]
@@ -123,12 +123,14 @@
         if i == 2:
             work.append((ready, 0.1, ("add", 0)))
     work += [(60.0, 0.1, ("add", i)) for i in range(1, len(groups))]
+    first_due = {("d", *s) for s in groups[1]}
     plan, now, got, events = [], 0.0, {}, events[::-1]
     plan += [("send", *s) for s in events.pop()[2]] + [("pass", "g", 0, 0), ("pass", "d", 0, 0)]
     while events or work:
         free = [item for item in work if item[0] <= now]
         soon = min([item[0] for item in work], default=1e9)
-        if events and events[-1][0] + margin <= (now if free else soon):
+        urgent = events and any((events[-1][1][0], *p[1:]) in first_due and got.get(("d", *p[1:]), 0) == 3 for p in events[-1][1][2])
+        if events and events[-1][0] + margin <= (now if free else soon) + (ahead if urgent else 0.0):
             t, what, sends = events.pop()
             plan.append(("recv", *what[:2]))
             now = max(now, t + margin)

time: 83.3 us -> 82.8 us (level)
  no operation moved by 1% of the time
where the time goes in v4:
time: 82.8 us; the launch traced here: 82.6 us
  Pallas kernels  81.7 us (99%)
  local copies, waits for them, and re-layouts  0.97 us (1%)
    pallas_call x1, Pallas kernels, per_device(): pl.pallas_call(kernel, out_shape=jax.ShapeDtypeStruct((TT, D), bf), in_sp...  81.7 us

profile of v4, /device:TPU:1, one launch (start us, length us, event | category | flops | bytes accessed | tf_op | source)
XLA Modules:
  0.0 82.6 jit_solution(14150560463299303012)
XLA Ops:
  0.0 81.7 %ffn.1 = bf16[256,2048]{1,0:T(8,128)(2,1)S(1)} custom-call(bf16[2048,2048]{1,0:T(8,128)(2,1)} %tok_hbm.1, f32[1,2048]{1,0:T(1,128)} %bitcast.5, bf16[704,128]{1,0:T(8,128)(2,1)} %bitcast.3, bf16[704,128]{1,0:T(8,128)(2,1)} %bitcast.4, bf16[704,128]{1,0:T(8,128)(2,1)} %dn_hbm.1), custom_call_target="tpu_custom_call" | custom-call | tf_op jit(solution)/shard_map/ffn/pallas_call | solution.py:381
  81.7 1.0 %copy.7 = bf16[256,2048]{1,0:T(8,128)(2,1)} copy(bf16[256,2048]{1,0:T(8,128)(2,1)S(1)} %ffn.1) | data formatting | bytes 2097152
